TPU v7x, 32 devices: a whole 2x2x4 slice. The times are simulated.
32 devices in a mesh: grp: 2 (over y), ep: 8 (over z, core), tp: 2 (over x).
Axes of the slice: x: 2, y: 2, z: 4, core: 2. Of those that a mesh axis runs over, the one named last changes fastest.
Arguments:
- tokens: bfloat16 [2048, 4096], P(('grp', 'ep'), 'tp'), parts along dimension 0, may hold values from -6 to 6
- routes: int32 [2048, 4], P(('grp', 'ep')), parts along dimension 0, may hold values from 0 to 7, all different within a row; in each aligned block of 128 rows (0 to 127, 128 to 255, ...) at most 128 rows name the same one
- route_weights: float32 [2048, 4], P(('grp', 'ep')), parts along dimension 0, may hold values from 0.1 to 1
- norm_gain: float32 [4096], replicated, may hold values from 0.1 to 1.9
- expert_gate: bfloat16 [8, 4096, 1024], P('ep', 'tp'), may hold values from -0.09375 to 0.09375
- expert_up: bfloat16 [8, 4096, 1024], P('ep', 'tp'), may hold values from -0.09375 to 0.09375
- expert_down: bfloat16 [8, 1024, 4096], P('ep', None, 'tp')
- shared_gate: bfloat16 [4096, 1024], P('tp'), may hold values from -0.09375 to 0.09375
- shared_up: bfloat16 [4096, 1024], P('tp'), may hold values from -0.09375 to 0.09375
- shared_down: bfloat16 [1024, 4096], P(None, 'tp')
- out_gain: float32 [4096], P('tp'), may hold values from 0.1 to 1.9
Outputs:
- layer_out: bfloat16 [2048, 4096], P(('grp', 'ep'), 'tp'), parts along dimension 0
There are 2 independent parts, one for each index of `grp`. A program takes and returns all parts, laid end to end along the dimension named above; an argument that names none is the same for every part. Nothing has to cross between parts.
Inputs may be any that keep to these rules, and one draw needn't show every extreme that they name: `routes`: each row names 4 different experts; among the rows of one index of ep no expert is named more than 128 times, and in some such block some expert is named exactly 128 times.
All inputs are finite; a program needn't handle non-finite values.
Results may differ from a plain program's by a relative error of at most 0.023.
Values may be sent and summed in bfloat16 or wider, within the bound.
A program may use at most 64 MiB of HBM per device.

v0:
```python
import jax
import jax.numpy as jnp
from jax import lax
from jax.sharding import PartitionSpec as P

epsilon = 1e-06


def local_product(source, matrix):
    return jnp.dot(source, matrix, preferred_element_type=jnp.float32)


def per_device(
    tokens,
    routes,
    route_weights,
    norm_gain,
    expert_gate,
    expert_up,
    expert_down,
    shared_gate,
    shared_up,
    shared_down,
    out_gain,
):
    block_width = tokens.shape[1]
    full_width = block_width * lax.axis_size("tp")
    width_index = lax.axis_index("tp")
    full_rows = lax.all_gather(tokens, "tp", axis=1, tiled=True)
    full_float = full_rows.astype(jnp.float32)
    normed_full = (
        full_float
        * lax.rsqrt(jnp.mean(full_float * full_float, axis=-1, keepdims=True) + epsilon)
        * norm_gain
    ).astype(jnp.bfloat16)
    normed_block = lax.dynamic_slice_in_dim(normed_full, width_index * block_width, block_width, 1)
    gate_matrix = expert_gate[0]
    up_matrix = expert_up[0]
    down_matrix = expert_down[0]
    experts = lax.axis_size("ep")
    choose = (routes[:, :, None] == jnp.arange(experts, dtype=jnp.int32)[None, None, :]).astype(
        jnp.float32
    )
    weight_table = jnp.sum(route_weights[:, :, None] * choose, axis=1)
    expert_input = lax.all_gather(normed_block, "ep", axis=0, tiled=True)
    table_all = lax.all_gather(weight_table, "ep", axis=0, tiled=True)
    summed = (
        lax.psum(local_product(expert_input, gate_matrix).astype(jnp.bfloat16), "tp").astype(
            jnp.float32
        ),
        lax.psum(local_product(expert_input, up_matrix).astype(jnp.bfloat16), "tp").astype(
            jnp.float32
        ),
        lax.psum(local_product(normed_block, shared_gate).astype(jnp.bfloat16), "tp").astype(
            jnp.float32
        ),
        lax.psum(local_product(normed_block, shared_up).astype(jnp.bfloat16), "tp").astype(
            jnp.float32
        ),
    )
    routed_hidden = (jax.nn.silu(summed[0]) * summed[1]).astype(jnp.bfloat16)
    shared_hidden = (jax.nn.silu(summed[2]) * summed[3]).astype(jnp.bfloat16)
    expert_rows = local_product(routed_hidden, down_matrix).astype(jnp.bfloat16)
    shared_out = local_product(shared_hidden, shared_down)
    own_expert = lax.axis_index("ep")
    column = lax.dynamic_slice_in_dim(table_all, own_expert, 1, 1)
    routed = lax.psum_scatter(
        (column * expert_rows.astype(jnp.float32)).astype(jnp.bfloat16),
        "ep",
        scatter_dimension=0,
        tiled=True,
    ).astype(jnp.float32)
    mixture = routed + shared_out
    square_sum = lax.psum(jnp.sum(mixture * mixture, axis=-1, keepdims=True), "tp")
    scale = lax.rsqrt(square_sum / full_width + epsilon)
    return (mixture * scale * out_gain).astype(jnp.bfloat16)


def solution(mesh):
    return jax.shard_map(
        per_device,
        mesh=mesh,
        in_specs=(
            P(("grp", "ep"), "tp"),
            P(("grp", "ep"), None),
            P(("grp", "ep"), None),
            P(),
            P("ep", "tp", None),
            P("ep", "tp", None),
            P("ep", None, "tp"),
            P("tp", None),
            P("tp", None),
            P(None, "tp"),
            P("tp"),
        ),
        out_specs=P(("grp", "ep"), "tp"),
        check_vma=False,
    )
```

profile of v0, /device:TPU:0, one launch (start us, length us, event | category | flops | bytes accessed | tf_op | source)
XLA Modules:
  0.0 293.4 jit_solution(16838798850096647116)
XLA Ops:
  6.5 0.0 all-gather.3.cloned.1.call-start
  6.5 0.7 all-gather.3.cloned.1.call-update
  7.3 0.0 all-gather.5.cloned.1.call-start
  7.3 0.0 dynamic-slice-start
  7.3 25.6 %all-gather.3.cloned.1.call-done = bf16[128,4096]{1,0:T(8,128)(2,1)} async-done(((bf16[128,2048]{1,0:T(8,128)(2,1)}), bf16[128,4096]{1,0:T(8,128)(2,1)}) %all-gather.3.cloned.1.call-update) | async-done | bytes 1048592 | tf_op jit(solution)/shard_map/all_gather | solution.py:29
  32.9 1.5 multiply_reduce_fusion
  34.4 1.4 convert_element_type.52
  35.9 0.0 dynamic-slice-done
  35.9 1.0 fusion.22
  36.8 0.0 all-gather.5.cloned.1.call-update
  36.9 0.0 all-reduce.3.cloned.1.call-start
  36.9 0.0 copy-start.1
  36.9 3.9 %convolution_convert_fusion = bf16[128,1024]{1,0:T(8,128)(2,1)} fusion(bf16[128,2048]{1,0:T(8,128)(2,1)} %fusion.22, bf16[2048,1024]{1,0:T(8,128)(2,1)} %param.19), kind=kOutput, calls=%fused_computation.19 | convolution fusion | flops 537001984 | bytes 4980736 | tf_op jit(solution)/shard_map/dot_general | solution.py:10
  40.8 0.0 copy-done
  40.9 1.5 convolution_convert_fusion.1
  42.3 41.6 %all-gather.5.cloned.1.call-done = bf16[1024,2048]{1,0:T(8,128)(2,1)} async-done(((bf16[128,2048]{1,0:T(8,128)(2,1)}), bf16[1024,2048]{1,0:T(8,128)(2,1)}) %all-gather.5.cloned.1.call-update) | async-done | bytes 4194320 | tf_op jit(solution)/shard_map/all_gather | solution.py:45
  83.9 9.5 %fusion.15 = bf16[1024,1024]{1,0:T(8,128)(2,1)} fusion(bf16[1024,2048]{1,0:T(8,128)(2,1)} %all-gather.5.cloned.1.call-done, bf16[1,2048,1024]{2,1,0:T(8,128)(2,1)} %param.15), kind=kOutput, calls=%fused_computation.17 | convolution fusion | flops 4296015872 | bytes 10485760 | tf_op jit(solution)/shard_map/dot_general | solution.py:10
  93.4 5.7 %fusion.18 = bf16[1024,1024]{1,0:T(8,128)(2,1)} fusion(bf16[1024,2048]{1,0:T(8,128)(2,1)S(1)} %copy-done.6, bf16[1,2048,1024]{2,1,0:T(8,128)(2,1)S(1)} %copy-done.5), kind=kOutput, calls=%fused_computation.18 | convolution fusion | flops 4296015872 | bytes 10485760 | tf_op jit(solution)/shard_map/dot_general | solution.py:10
  99.1 0.0 all-reduce.3.cloned.1.call-update
  99.1 0.0 reduce-scatter.2.cloned.1.call-start
  99.2 0.6 copy-done.3
  99.8 0.0 copy-done.4
  99.8 14.1 %all_gather.9 = f32[1024,8]{0,1:T(8,128)S(1)} all-gather(f32[128,8]{0,1:T(8,128)S(1)} %select_reduce_fusion), channel_id=1, replica_groups=mesh['grp'=2,'ep'=8,'tp'=2] {'ep'}, dimensions={0}, use_global_device_ids=true | all-gather | bytes 36864 | tf_op jit(solution)/shard_map/all_gather | solution.py:46
  113.9 103.5 %all-reduce.3.cloned.1.call-done = (bf16[1024,1024]{1,0:T(8,128)(2,1)}, bf16[1024,1024]{1,0:T(8,128)(2,1)}, bf16[128,1024]{1,0:T(8,128)(2,1)}, bf16[128,1024]{1,0:T(8,128)(2,1)}) async-done(((bf16[1024,1024]{1,0:T(8,128)(2,1)}, bf16[1024,1024]{1,0:T(8,128)(2,1)}, bf16[128,1024]{1,0:T(8,128)(2,1)}, bf16[128,1024]{1,0:T(8,128)(2,1)}), (bf16[1024,1024]{1,0:T(8,128)(2,1)}, bf16[1024,1024]{1,0:T(8,128)(2,1)}, ...) | async-done | bytes 4718608 | tf_op jit(solution)/shard_map/psum | solution.py:51
  217.4 10.3 %multiply_convert_fusion = bf16[1024,2048]{1,0:T(8,128)(2,1)} fusion(f32[1024]{0:T(1024)S(1)} %bitcast.26, bf16[1,1024,2048]{2,1,0:T(8,128)(2,1)} %param.17, bf16[1024,1024]{1,0:T(8,128)(2,1)} %get-tuple-element.5, bf16[1024,1024]{1,0:T(8,128)(2,1)} %get-tuple-element.6), kind=kOutput, calls=%fused_computation | convolution fusion | flops 4311744512 | bytes 12587008 | tf_op jit(solution)/shard_map/dot_general | solution.py:10
  227.7 0.0 reduce-scatter.2.cloned.1.call-update
  227.7 0.0 copy-start.2
  227.7 50.1 %reduce-scatter.2.cloned.1.call-done = bf16[128,2048]{1,0:T(8,128)(2,1)} async-done(((bf16[1024,2048]{1,0:T(8,128)(2,1)}), bf16[128,2048]{1,0:T(8,128)(2,1)}) %reduce-scatter.2.cloned.1.call-update) | async-done | bytes 524304 | tf_op jit(solution)/shard_map/reduce_scatter | solution.py:67
  277.8 0.0 copy-done.7
  277.8 3.2 %multiply_reduce_fusion.1 = (f32[128]{0:T(128)S(1)}, f32[128,2048]{1,0:T(8,128)S(1)}) fusion(bf16[1024,2048]{1,0:T(8,128)(2,1)} %param.20, bf16[128,1024]{1,0:T(8,128)(2,1)S(1)} %copy-done.7, bf16[128,1024]{1,0:T(8,128)(2,1)S(1)} %copy-done.8, bf16[128,2048]{1,0:T(8,128)(2,1)} %reduce-scatter.2.cloned.1.call-done), kind=kOutput, calls=%fused_computation.25 | convolution fusion | flops 538967936 | bytes 6291968 | tf_op jit(solution)/shard_map/dot_general | solution.py:10
  281.0 4.9 %psum.39 = f32[128,1]{0,1:T(1,128)S(1)} all-reduce(f32[128,1]{0,1:T(1,128)S(1)} %bitcast.27), channel_id=1, replica_groups=mesh['grp'=2,'ep'=8,'tp'=2] {'tp'}, use_global_device_ids=true, to_apply=%region_8.9 | all-reduce | flops 128 | bytes 1024 | tf_op jit(solution)/shard_map/psum | solution.py:74
  286.0 1.0 multiply_convert_fusion.1
  (16 shorter events, 0.1 us)
Async XLA Ops:
  6.5 26.4 %all-gather.3.cloned.1.call-start = ((), (), s32[]{:S(2)}) async-start(), calls=%async_computation.1 | async-start | bytes 1572864 | tf_op jit(solution)/shard_map/all_gather | solution.py:29
  7.3 76.6 %all-gather.5.cloned.1.call-start = ((), (), s32[]{:S(2)}) async-start(), calls=%async_computation.2 | async-start | bytes 4718592 | tf_op jit(solution)/shard_map/all_gather | solution.py:45
  7.3 28.6 %dynamic-slice-start = ((f32[4096]{0:T(1024)}, s32[]{:T(128)}), f32[2048]{0:T(1024)S(1)}, s32[]{:S(2)}) async-start(f32[4096]{0:T(1024)} %param.14, s32[]{:T(128)} %select_n.7), calls=%async_computation.5 | async-start | bytes 16896 | tf_op jit(solution)/shard_map/dynamic_slice | solution.py:36
  36.8 4.0 %copy-start = (bf16[128,2048]{1,0:T(8,128)(2,1)S(1)}, bf16[128,2048]{1,0:T(8,128)(2,1)}, u32[]{:S(2)}) copy-start(bf16[128,2048]{1,0:T(8,128)(2,1)} %fusion.22) | copy-start | bytes 1572868
  36.9 180.5 %all-reduce.3.cloned.1.call-start = ((), (), s32[]{:S(2)}) async-start(), calls=%async_computation.4 | async-start | bytes 9437184 | tf_op jit(solution)/shard_map/psum | solution.py:51
  36.9 3.9 %copy-start.1 = (bf16[2048,1024]{1,0:T(8,128)(2,1)S(1)}, bf16[2048,1024]{1,0:T(8,128)(2,1)}, u32[]{:S(2)}) copy-start(bf16[2048,1024]{1,0:T(8,128)(2,1)} %param.18) | copy-start | bytes 12582916
  83.9 9.5 %copy-start.5 = (bf16[1,2048,1024]{2,1,0:T(8,128)(2,1)S(1)}, bf16[1,2048,1024]{2,1,0:T(8,128)(2,1)}, u32[]{:S(2)}) copy-start(bf16[1,2048,1024]{2,1,0:T(8,128)(2,1)} %param.16) | copy-start | bytes 12582916
  83.9 9.5 %copy-start.6 = (bf16[1024,2048]{1,0:T(8,128)(2,1)S(1)}, bf16[1024,2048]{1,0:T(8,128)(2,1)}, u32[]{:S(2)}) copy-start(bf16[1024,2048]{1,0:T(8,128)(2,1)} %all-gather.5.cloned.1.call-done) | copy-start | bytes 12582916
  99.1 0.7 copy-start.3
  99.1 0.7 copy-start.4
  99.1 178.7 %reduce-scatter.2.cloned.1.call-start = ((), (), s32[]{:S(2)}) async-start(), calls=%async_computation.3 | async-start | bytes 4718592 | tf_op jit(solution)/shard_map/reduce_scatter | solution.py:67
  227.7 50.1 %copy-start.7 = (bf16[128,1024]{1,0:T(8,128)(2,1)S(1)}, bf16[128,1024]{1,0:T(8,128)(2,1)}, u32[]{:S(2)}) copy-start(bf16[128,1024]{1,0:T(8,128)(2,1)} %get-tuple-element.7) | copy-start | bytes 786436
  227.7 50.1 %copy-start.8 = (bf16[128,1024]{1,0:T(8,128)(2,1)S(1)}, bf16[128,1024]{1,0:T(8,128)(2,1)}, u32[]{:S(2)}) copy-start(bf16[128,1024]{1,0:T(8,128)(2,1)} %get-tuple-element.8) | copy-start | bytes 786436
  227.7 58.2 %copy-start.2 = (f32[2048]{0:T(1024)S(1)}, f32[2048]{0:T(1024)}, u32[]{:S(2)}) copy-start(f32[2048]{0:T(1024)} %param.21) | copy-start | bytes 24580
Sparse Core Ops, SparseCore 0:
  8.9 23.9 all-gather.2
  37.0 46.8 all-gather.4
  99.3 118.0 all-reduce.2
  227.8 49.9 reduce-scatter.1
where the time goes:
time: 294 us; the launch traced here: 293 us
  waiting for transfers between devices  221 us (75%)
  matrix products  34.1 us (12%)
  blocking collectives  19 us (6%)
  between operations  13.2 us (4%)
  other arithmetic  4.88 us (2%)
    psum x1, waiting for transfers between devices, per_device(): lax.psum(local_product(expert_input, up_matrix).astype(jnp.bfloat16), 'tp')  103 us
    reduce_scatter x1, waiting for transfers between devices, per_device(): lax.psum_scatter((column * expert_rows.astype(jnp.float32)).astype(jnp.bf...  50.1 us
    all_gather x1, waiting for transfers between devices, per_device(): expert_input = lax.all_gather(normed_block, 'ep', axis=0, tiled=True)  41.6 us
    dot_general x6, matrix products, local_product(): return jnp.dot(source, matrix, preferred_element_type=jnp.float32)  34.1 us
    all_gather x1, waiting for transfers between devices, per_device(): full_rows = lax.all_gather(tokens, 'tp', axis=1, tiled=True)  25.6 us
    all_gather x1, blocking collectives, per_device(): table_all = lax.all_gather(weight_table, 'ep', axis=0, tiled=True)  14.1 us
  transfers between devices with their start and end apart: 4, of which 4 were waited for; matrix products, arithmetic and copies ran while one was open for 2% of the time, Pallas kernels for 0%

commit v1 on v0

--- a/solution.py
+++ b/solution.py
@@ -26,7 +26,7 @@
     block_width = tokens.shape[1]
     full_width = block_width * lax.axis_size("tp")
     width_index = lax.axis_index("tp")
-    full_rows = lax.all_gather(tokens, "tp", axis=1, tiled=True)
+    full_rows = jnp.concatenate(lax.all_gather(tokens, "tp"), axis=1)
     full_float = full_rows.astype(jnp.float32)
     normed_full = (
         full_float

time: 294 us -> 296 us (level)
  no operation moved by 1% of the time
where the time goes in v1:
time: 296 us
  waiting for transfers between devices  222 us (75%)
  matrix products  34.3 us (12%)
  blocking collectives  19.2 us (6%)
  between operations  13.2 us (4%)
  other arithmetic  5.17 us (2%)
    psum x1, waiting for transfers between devices, per_device(): lax.psum(local_product(expert_input, up_matrix).astype(jnp.bfloat16), 'tp')  103 us
    reduce_scatter x1, waiting for transfers between devices, per_device(): lax.psum_scatter((column * expert_rows.astype(jnp.float32)).astype(jnp.bf...  50.1 us
    all_gather x1, waiting for transfers between devices, per_device(): expert_input = lax.all_gather(normed_block, 'ep', axis=0, tiled=True)  42.5 us
    dot_general x6, matrix products, local_product(): return jnp.dot(source, matrix, preferred_element_type=jnp.float32)  34.3 us
    all_gather x1, waiting for transfers between devices, per_device(): full_rows = jnp.concatenate(lax.all_gather(tokens, 'tp'), axis=1)  25.6 us
    all_gather x1, blocking collectives, per_device(): table_all = lax.all_gather(weight_table, 'ep', axis=0, tiled=True)  14.3 us
  transfers between devices with their start and end apart: 4, of which 4 were waited for; matrix products, arithmetic and copies ran while one was open for 2% of the time, Pallas kernels for 0%

profile of v1, /device:TPU:0, one launch (start us, length us, event | category | flops | bytes accessed | tf_op | source)
XLA Modules:
  0.0 296.1 jit_solution(13095597433880072832)
XLA Ops:
  6.5 0.0 all-gather.6.cloned.1.call-start
  6.5 0.7 all-gather.6.cloned.1.call-update
  7.3 0.0 all-gather.4.cloned.1.call-start
  7.3 0.0 dynamic-slice-start
  7.3 25.6 %all-gather.6.cloned.1.call-done = bf16[256,2048]{1,0:T(8,128)(2,1)} async-done(((bf16[128,2048]{1,0:T(8,128)(2,1)}), bf16[256,2048]{1,0:T(8,128)(2,1)}) %all-gather.6.cloned.1.call-update) | async-done | bytes 1048592 | tf_op jit(solution)/shard_map/all_gather | solution.py:29
  32.9 1.5 convert_bitcast_fusion
  34.5 1.9 copy.19
  36.3 0.0 copy-done.1
  36.3 0.3 fusion.14
  36.6 2.4 fusion.23
  39.0 0.0 all-gather.4.cloned.1.call-update
  39.0 0.0 all-reduce.3.cloned.1.call-start
  39.1 0.0 copy-start.2
  39.1 3.9 %convolution_convert_fusion = bf16[128,1024]{1,0:T(8,128)(2,1)} fusion(bf16[128,2048]{0,1:T(8,128)(2,1)} %fusion.23, bf16[2048,1024]{1,0:T(8,128)(2,1)} %param.19), kind=kOutput, calls=%fused_computation.21 | convolution fusion | flops 537001984 | bytes 4980736 | tf_op jit(solution)/shard_map/dot_general | solution.py:10
  43.0 1.5 convolution_convert_fusion.1
  44.5 42.5 %all-gather.4.cloned.1.call-done = bf16[1024,2048]{0,1:T(8,128)(2,1)} async-done(((bf16[128,2048]{0,1:T(8,128)(2,1)}), bf16[1024,2048]{0,1:T(8,128)(2,1)}) %all-gather.4.cloned.1.call-update) | async-done | bytes 4194320 | tf_op jit(solution)/shard_map/all_gather | solution.py:45
  87.0 9.6 %fusion.16 = bf16[1024,1024]{1,0:T(8,128)(2,1)} fusion(bf16[1024,2048]{0,1:T(8,128)(2,1)} %all-gather.4.cloned.1.call-done, bf16[1,2048,1024]{2,1,0:T(8,128)(2,1)} %param.15), kind=kOutput, calls=%fused_computation.19 | convolution fusion | flops 4296015872 | bytes 10485760 | tf_op jit(solution)/shard_map/dot_general | solution.py:10
  96.6 5.8 %fusion.19 = bf16[1024,1024]{1,0:T(8,128)(2,1)} fusion(bf16[1024,2048]{0,1:T(8,128)(2,1)S(1)} %copy-done.7, bf16[1,2048,1024]{2,1,0:T(8,128)(2,1)S(1)} %copy-done.6), kind=kOutput, calls=%fused_computation.20 | convolution fusion | flops 4296015872 | bytes 10485760 | tf_op jit(solution)/shard_map/dot_general | solution.py:10
  102.4 0.0 all-reduce.3.cloned.1.call-update
  102.4 0.0 reduce-scatter.2.cloned.1.call-start
  102.5 0.6 copy-done.4
  103.1 0.0 copy-done.5
  103.1 14.3 %all_gather.12 = f32[1024,8]{0,1:T(8,128)S(1)} all-gather(f32[128,8]{0,1:T(8,128)S(1)} %select_reduce_fusion), channel_id=1, replica_groups=mesh['grp'=2,'ep'=8,'tp'=2] {'ep'}, dimensions={0}, use_global_device_ids=true | all-gather | bytes 36864 | tf_op jit(solution)/shard_map/all_gather | solution.py:46
  117.4 102.7 %all-reduce.3.cloned.1.call-done = (bf16[1024,1024]{1,0:T(8,128)(2,1)}, bf16[1024,1024]{1,0:T(8,128)(2,1)}, bf16[128,1024]{1,0:T(8,128)(2,1)}, bf16[128,1024]{1,0:T(8,128)(2,1)}) async-done(((bf16[1024,1024]{1,0:T(8,128)(2,1)}, bf16[1024,1024]{1,0:T(8,128)(2,1)}, bf16[128,1024]{1,0:T(8,128)(2,1)}, bf16[128,1024]{1,0:T(8,128)(2,1)}), (bf16[1024,1024]{1,0:T(8,128)(2,1)}, bf16[1024,1024]{1,0:T(8,128)(2,1)}, ...) | async-done | bytes 4718608 | tf_op jit(solution)/shard_map/psum | solution.py:51
  220.0 10.3 %multiply_convert_fusion = bf16[1024,2048]{1,0:T(8,128)(2,1)} fusion(f32[1024]{0:T(1024)S(1)} %bitcast.34, bf16[1,1024,2048]{2,1,0:T(8,128)(2,1)} %param.17, bf16[1024,1024]{1,0:T(8,128)(2,1)} %get-tuple-element.5, bf16[1024,1024]{1,0:T(8,128)(2,1)} %get-tuple-element.6), kind=kOutput, calls=%fused_computation | convolution fusion | flops 4311744512 | bytes 12587008 | tf_op jit(solution)/shard_map/dot_general | solution.py:10
  230.4 0.0 reduce-scatter.2.cloned.1.call-update
  230.4 0.0 copy-start.3
  230.4 50.1 %reduce-scatter.2.cloned.1.call-done = bf16[128,2048]{1,0:T(8,128)(2,1)} async-done(((bf16[1024,2048]{1,0:T(8,128)(2,1)}), bf16[128,2048]{1,0:T(8,128)(2,1)}) %reduce-scatter.2.cloned.1.call-update) | async-done | bytes 524304 | tf_op jit(solution)/shard_map/reduce_scatter | solution.py:67
  280.5 3.2 %multiply_reduce_fusion = (f32[128]{0:T(128)S(1)}, f32[128,2048]{1,0:T(8,128)S(1)}) fusion(bf16[1024,2048]{1,0:T(8,128)(2,1)} %param.20, bf16[128,1024]{1,0:T(8,128)(2,1)S(1)} %copy-done.8, bf16[128,1024]{1,0:T(8,128)(2,1)S(1)} %copy-done.9, bf16[128,2048]{1,0:T(8,128)(2,1)} %reduce-scatter.2.cloned.1.call-done), kind=kOutput, calls=%fused_computation.27 | convolution fusion | flops 538967936 | bytes 6291968 | tf_op jit(solution)/shard_map/dot_general | solution.py:10
  283.7 4.9 %psum.39 = f32[128,1]{0,1:T(1,128)S(1)} all-reduce(f32[128,1]{0,1:T(1,128)S(1)} %bitcast.35), channel_id=1, replica_groups=mesh['grp'=2,'ep'=8,'tp'=2] {'tp'}, use_global_device_ids=true, to_apply=%region_8.9 | all-reduce | flops 128 | bytes 1024 | tf_op jit(solution)/shard_map/psum | solution.py:74
  288.6 0.0 copy-done.3
  288.6 1.0 multiply_convert_fusion.1
  (19 shorter events, 0.1 us)
Async XLA Ops:
  6.5 26.4 %all-gather.6.cloned.1.call-start = ((), (), s32[]{:S(2)}) async-start(), calls=%async_computation.3 | async-start | bytes 1572864 | tf_op jit(solution)/shard_map/all_gather | solution.py:29
  7.3 79.7 %all-gather.4.cloned.1.call-start = ((), (), s32[]{:S(2)}) async-start(), calls=%async_computation.1 | async-start | bytes 4718592 | tf_op jit(solution)/shard_map/all_gather | solution.py:45
  7.3 29.3 %dynamic-slice-start = ((f32[4096]{0:T(1024)}, s32[]{:T(128)}), f32[2048]{0:T(1024)S(1)}, s32[]{:S(2)}) async-start(f32[4096]{0:T(1024)} %param.14, s32[]{:T(128)} %select_n.7), calls=%async_computation.5 | async-start | bytes 16896 | tf_op jit(solution)/shard_map/dynamic_slice | solution.py:36
  32.9 3.4 %copy-start.1 = (bf16[256,2048]{1,0:T(8,128)(2,1)S(1)}, bf16[256,2048]{1,0:T(8,128)(2,1)}, u32[]{:S(2)}) copy-start(bf16[256,2048]{1,0:T(8,128)(2,1)} %all-gather.6.cloned.1.call-done) | copy-start | bytes 3145732
  39.0 4.0 %copy-start = (bf16[128,2048]{0,1:T(8,128)(2,1)S(1)}, bf16[128,2048]{0,1:T(8,128)(2,1)}, u32[]{:S(2)}) copy-start(bf16[128,2048]{0,1:T(8,128)(2,1)} %fusion.23) | copy-start | bytes 1572868
  39.0 181.0 %all-reduce.3.cloned.1.call-start = ((), (), s32[]{:S(2)}) async-start(), calls=%async_computation.4 | async-start | bytes 9437184 | tf_op jit(solution)/shard_map/psum | solution.py:51
  39.1 4.0 %copy-start.2 = (bf16[2048,1024]{1,0:T(8,128)(2,1)S(1)}, bf16[2048,1024]{1,0:T(8,128)(2,1)}, u32[]{:S(2)}) copy-start(bf16[2048,1024]{1,0:T(8,128)(2,1)} %param.18) | copy-start | bytes 12582916
  87.0 9.6 %copy-start.6 = (bf16[1,2048,1024]{2,1,0:T(8,128)(2,1)S(1)}, bf16[1,2048,1024]{2,1,0:T(8,128)(2,1)}, u32[]{:S(2)}) copy-start(bf16[1,2048,1024]{2,1,0:T(8,128)(2,1)} %param.16) | copy-start | bytes 12582916
  87.0 9.6 %copy-start.7 = (bf16[1024,2048]{0,1:T(8,128)(2,1)S(1)}, bf16[1024,2048]{0,1:T(8,128)(2,1)}, u32[]{:S(2)}) copy-start(bf16[1024,2048]{0,1:T(8,128)(2,1)} %all-gather.4.cloned.1.call-done) | copy-start | bytes 12582916
  102.4 0.7 copy-start.4
  102.4 0.7 copy-start.5
  102.4 178.1 %reduce-scatter.2.cloned.1.call-start = ((), (), s32[]{:S(2)}) async-start(), calls=%async_computation.2 | async-start | bytes 4718592 | tf_op jit(solution)/shard_map/reduce_scatter | solution.py:67
  230.4 50.1 %copy-start.8 = (bf16[128,1024]{1,0:T(8,128)(2,1)S(1)}, bf16[128,1024]{1,0:T(8,128)(2,1)}, u32[]{:S(2)}) copy-start(bf16[128,1024]{1,0:T(8,128)(2,1)} %get-tuple-element.7) | copy-start | bytes 786436
  230.4 50.1 %copy-start.9 = (bf16[128,1024]{1,0:T(8,128)(2,1)S(1)}, bf16[128,1024]{1,0:T(8,128)(2,1)}, u32[]{:S(2)}) copy-start(bf16[128,1024]{1,0:T(8,128)(2,1)} %get-tuple-element.8) | copy-start | bytes 786436
  230.4 58.2 %copy-start.3 = (f32[2048]{0:T(1024)S(1)}, f32[2048]{0:T(1024)}, u32[]{:S(2)}) copy-start(f32[2048]{0:T(1024)} %param.21) | copy-start | bytes 24580
Sparse Core Ops, SparseCore 0:
  8.9 23.9 all-gather.5
  39.1 47.8 all-gather.3
  102.5 117.4 all-reduce.2
  230.5 49.9 reduce-scatter.1
